TPU v7x, 32 devices: a whole 2x2x4 slice. The times are simulated.
32 devices in a mesh: fs: 8 (over z, x), tp: 4 (over y, core).
Axes of the slice: x: 2, y: 2, z: 4, core: 2. Of those that a mesh axis runs over, the one named last changes fastest.
Arguments:
- normed_input: bfloat16 [8192, 2048], P('fs'), may hold values from -64 to 64
- query_cotangent: bfloat16 [8192, 1024], P('fs', 'tp'), may hold values from -6 to 6
- key_cotangent: bfloat16 [8192, 512], P('fs', 'tp'), may hold values from -6 to 6
- query_weight: float32 [2048, 1024], P('fs', 'tp'), may hold values from -6 to 6
- key_weight: float32 [2048, 512], P('fs', 'tp'), may hold values from -6 to 6
- query_basis: bfloat16 [1024, 128], P('tp'), may hold values from -1 to 1
- key_basis: bfloat16 [512, 128], P('tp'), may hold values from -1 to 1
- moment_mean: float32 [2, 2048, 128], P(None, 'fs'), may hold values from -3 to 3
- moment_square: float32 [2, 2048, 128], P(None, 'fs'), may hold values from 0.25 to 4
Outputs:
- query_step: float32 [2048, 1024], P('fs', 'tp')
- key_step: float32 [2048, 512], P('fs', 'tp')
- query_updated: float32 [2048, 1024], P('fs', 'tp')
- key_updated: float32 [2048, 512], P('fs', 'tp')
- query_copy: bfloat16 [2048, 1024], P('fs', 'tp')
- key_copy: bfloat16 [2048, 512], P('fs', 'tp')
- mean_updated: float32 [2, 2048, 128], P(None, 'fs')
- square_updated: float32 [2, 2048, 128], P(None, 'fs')
All inputs are finite; a program needn't handle non-finite values.
Results may differ from a plain program's by a relative error of at most 0.0011.
Values sent between devices are 32-bit elements; how exact they have to be, the bound alone decides.
A program may use at most 64 MiB of HBM per device.

v0:
```python
import jax
import jax.numpy as jnp
from jax import lax
from jax.sharding import PartitionSpec as P

BETA_MEAN = 0.75
BETA_SQUARE = 0.8
STEP_RATE = 0.25
EPSILON = 1e-06


def local(
    normed_input,
    query_cotangent,
    key_cotangent,
    query_weight,
    key_weight,
    query_basis,
    key_basis,
    moment_mean,
    moment_square,
):
    highest = lax.Precision.HIGHEST
    contract = (((0,), (0,)), ((), ()))
    row_count = query_weight.shape[0]
    rank_width = query_basis.shape[1]
    query_float = query_basis.astype(jnp.float32)
    key_float = key_basis.astype(jnp.float32)
    partial_precision = lax.Precision.HIGH
    query_part = lax.dot_general(
        normed_input, query_cotangent, contract, preferred_element_type=jnp.float32
    )
    key_part = lax.dot_general(
        normed_input, key_cotangent, contract, preferred_element_type=jnp.float32
    )
    query_part, key_part = (query_part, key_part)
    summed = lax.psum_scatter(
        jnp.concatenate(
            [
                jnp.dot(query_part, query_float, precision=partial_precision),
                jnp.dot(key_part, key_float, precision=partial_precision),
            ],
            axis=1,
        ),
        "fs",
        scatter_dimension=0,
        tiled=True,
    )
    query_projected = summed[:, :rank_width]
    key_projected = summed[:, rank_width:]
    projected = lax.psum(jnp.stack([query_projected, key_projected]), "tp")
    total_square = lax.psum(jnp.sum(projected * projected), "fs")
    entry_count = 2.0 * row_count * lax.axis_size("fs") * rank_width
    normalized = projected * lax.rsqrt(total_square / entry_count + EPSILON)
    mean_updated = BETA_MEAN * moment_mean + (1.0 - BETA_MEAN) * normalized
    square_updated = BETA_SQUARE * moment_square + (1.0 - BETA_SQUARE) * normalized * normalized
    direction = mean_updated / jnp.sqrt(square_updated)
    outer = (((1,), (1,)), ((), ()))
    query_step = lax.dot_general(direction[0], query_float, outer, precision=highest)
    key_step = lax.dot_general(direction[1], key_float, outer, precision=highest)
    query_updated = query_weight - STEP_RATE * query_step
    key_updated = key_weight - STEP_RATE * key_step
    return (
        query_step,
        key_step,
        query_updated,
        key_updated,
        query_updated.astype(jnp.bfloat16),
        key_updated.astype(jnp.bfloat16),
        mean_updated,
        square_updated,
    )


def solution(mesh):
    in_specs = (
        P("fs", None),
        P("fs", "tp"),
        P("fs", "tp"),
        P("fs", "tp"),
        P("fs", "tp"),
        P("tp", None),
        P("tp", None),
        P(None, "fs", None),
        P(None, "fs", None),
    )
    out_specs = (
        P("fs", "tp"),
        P("fs", "tp"),
        P("fs", "tp"),
        P("fs", "tp"),
        P("fs", "tp"),
        P("fs", "tp"),
        P(None, "fs", None),
        P(None, "fs", None),
    )
    return jax.shard_map(local, mesh=mesh, in_specs=in_specs, out_specs=out_specs, check_vma=False)
```

profile of v0, /device:TPU:0, one launch (start us, length us, event | category | flops | bytes accessed | tf_op | source)
XLA Modules:
  0.0 158.6 jit_solution(541091675263221760)
XLA Ops:
  7.2 0.0 copy-start
  7.2 0.0 copy-start.2
  7.2 0.0 reduce-scatter.2.cloned.1.call-start
  7.2 1.0 copy-done
  8.2 0.0 copy-start.1
  8.2 3.7 %fusion.6 = f32[2048,256]{1,0:T(8,128)S(1)} fusion(bf16[1024,2048]{1,0:T(8,128)(2,1)} %param.9, bf16[1024,256]{1,0:T(8,128)(2,1)S(1)} %copy-done), kind=kOutput, calls=%fused_computation.17 | convolution fusion | flops 1073741824 | bytes 6815744 | tf_op jit(solution)/shard_map/dot_general | solution.py:30
  11.9 0.0 copy-done.2
  11.9 0.0 copy-done.1
  11.9 0.0 copy-start.4
  11.9 1.3 fusion.8
  13.2 0.0 copy-done.4
  13.3 0.0 copy-start.7
  13.3 0.8 fusion.7
  14.1 0.0 copy-done.7
  14.1 0.5 fusion.9
  14.6 1.5 pad_maximum_fusion
  16.1 0.0 copy-start.5
  16.1 0.0 copy-start.6
  16.1 0.0 reduce-scatter.2.cloned.1.call-update
  16.1 0.0 copy-start.3
  16.2 0.0 all-reduce.2.cloned.1.call-start
  16.2 72.0 %reduce-scatter.2.cloned.1.call-done = f32[256,256]{0,1:T(8,128)} async-done(((f32[2048,256]{0,1:T(8,128)}), f32[256,256]{0,1:T(8,128)}) %reduce-scatter.2.cloned.1.call-update) | async-done | bytes 262160 | tf_op jit(solution)/shard_map/reduce_scatter | solution.py:37
  88.2 1.0 slice_bitcast_fusion.5
  89.2 0.7 pad_maximum_fusion.1
  89.9 0.0 copy-start.8
  89.9 0.0 all-reduce.2.cloned.1.call-update
  89.9 0.0 copy-done.5
  89.9 0.1 copy.17
  90.0 32.4 %all-reduce.2.cloned.1.call-done = f32[2,256,128]{1,2,0:T(8,128)} async-done(((f32[2,256,128]{1,2,0:T(8,128)}), f32[2,256,128]{1,2,0:T(8,128)}) %all-reduce.2.cloned.1.call-update) | async-done | bytes 262160 | tf_op jit(solution)/shard_map/psum | solution.py:51
  122.4 1.6 %multiply_reduce_fusion = f32[]{:T(128)} fusion(f32[2,256,128]{1,2,0:T(8,128)} %all-reduce.2.cloned.1.call-done), kind=kLoop, calls=%fused_computation.7 | loop fusion | flops 131071 | bytes 262148 | tf_op jit(solution)/shard_map/reduce_sum | solution.py:52
  124.1 0.0 copy-done.6
  124.1 0.1 copy.18
  124.2 22.0 %psum.15 = f32[]{:T(128)} all-reduce(f32[]{:T(128)} %multiply_reduce_fusion), channel_id=1, replica_groups=mesh['fs'=8,'tp'=4] {'fs'}, use_global_device_ids=true, to_apply=%region_3.0 | all-reduce | flops 1 | bytes 8 | tf_op jit(solution)/shard_map/psum | solution.py:52
  146.9 1.0 rsqrt_multiply_fusion
  147.9 0.0 copy-done.3
  147.9 1.1 fusion.4
  149.1 0.0 copy-done.8
  149.1 1.0 fusion.3
  150.1 0.8 copy.19
  150.9 0.8 copy.20
Async XLA Ops:
  7.2 1.0 copy-start
  7.2 4.7 %copy-start.2 = (bf16[1024,128]{1,0:T(8,128)(2,1)S(1)}, bf16[1024,128]{1,0:T(8,128)(2,1)}, u32[]{:S(2)}) copy-start(bf16[1024,128]{1,0:T(8,128)(2,1)} %param.11) | copy-start | bytes 786436
  7.2 81.0 %reduce-scatter.2.cloned.1.call-start = ((), (), s32[]{:S(2)}) async-start(), calls=%async_computation.1 | async-start | bytes 2359296 | tf_op jit(solution)/shard_map/reduce_scatter | solution.py:37
  8.2 3.7 %copy-start.1 = (bf16[1024,2048]{1,0:T(8,128)(2,1)S(1)}, bf16[1024,2048]{1,0:T(8,128)(2,1)}, u32[]{:S(2)}) copy-start(bf16[1024,2048]{1,0:T(8,128)(2,1)} %param.9) | copy-start | bytes 12582916
  11.9 1.3 copy-start.4
  13.3 0.9 copy-start.7
  16.1 73.8 %copy-start.5 = (f32[2,256,128]{2,1,0:T(8,128)S(1)}, f32[2,256,128]{2,1,0:T(8,128)}, u32[]{:S(2)}) copy-start(f32[2,256,128]{2,1,0:T(8,128)} %param.16) | copy-start | bytes 786436
  16.1 107.9 %copy-start.6 = (f32[2,256,128]{2,1,0:T(8,128)S(1)}, f32[2,256,128]{2,1,0:T(8,128)}, u32[]{:S(2)}) copy-start(f32[2,256,128]{2,1,0:T(8,128)} %param.17) | copy-start | bytes 786436
  16.1 131.8 %copy-start.3 = (f32[256,256]{1,0:T(8,128)S(1)}, f32[256,256]{1,0:T(8,128)}, u32[]{:S(2)}) copy-start(f32[256,256]{1,0:T(8,128)} %param.12) | copy-start | bytes 786436
  16.2 106.3 %all-reduce.2.cloned.1.call-start = ((), (), s32[]{:S(2)}) async-start(), calls=%async_computation.2 | async-start | bytes 524288 | tf_op jit(solution)/shard_map/psum | solution.py:51
  89.9 59.2 %copy-start.8 = (f32[256,128]{1,0:T(8,128)S(1)}, f32[256,128]{1,0:T(8,128)}, u32[]{:S(2)}) copy-start(f32[256,128]{1,0:T(8,128)} %param.13) | copy-start | bytes 393220
Sparse Core Ops, SparseCore 0:
  16.3 71.8 reduce-scatter.1
  91.1 31.3 all-reduce.1
where the time goes:
time: 159 us
  waiting for transfers between devices  104 us (65%)
  blocking collectives  22 us (14%)
  between operations  14.9 us (9%)
  matrix products  8.46 us (5%)
  other arithmetic  4.88 us (3%)
  local copies, waits for them, and re-layouts  3.93 us (2%)
    reduce_scatter x1, waiting for transfers between devices, local(): lax.psum_scatter(jnp.concatenate([jnp.dot(query_part, query_float, precis...  72 us
    psum x1, waiting for transfers between devices, local(): projected = lax.psum(jnp.stack([query_projected, key_projected]), 'tp')  32.4 us
    psum x1, blocking collectives, local(): total_square = lax.psum(jnp.sum(projected * projected), 'fs')  22 us
    dot_general x1, matrix products, local(): lax.dot_general(normed_input, query_cotangent, contract, preferred_elemen...  3.68 us
  transfers between devices with their start and end apart: 2, of which 2 were waited for; matrix products, arithmetic and copies ran while one was open for 0% of the time, Pallas kernels for 0%

commit v1 on v0

--- a/solution.py
+++ b/solution.py
@@ -48,7 +48,7 @@
     )
     query_projected = summed[:, :rank_width]
     key_projected = summed[:, rank_width:]
-    projected = lax.psum(jnp.stack([query_projected, key_projected]), "tp")
+    projected = jnp.sum(lax.all_gather(jnp.stack([query_projected, key_projected]), "tp"), axis=0)
     total_square = lax.psum(jnp.sum(projected * projected), "fs")
     entry_count = 2.0 * row_count * lax.axis_size("fs") * rank_width
     normalized = projected * lax.rsqrt(total_square / entry_count + EPSILON)

time: 159 us -> 142 us (0.89)
  waiting for transfers between devices: 104 us -> 87.8 us
    psum x1 -> x0, waiting for transfers between devices: 32.4 us -> none  [local(): projected = lax.psum(jnp.stack([query_projected, key_projected]), 'tp')]
    all_gather x0 -> x1, waiting for transfers between devices: none -> 15.9 us  [local(): lax.all_gather(jnp.stack([query_projected, key_projected]), 'tp')]
where the time goes in v1:
time: 142 us
  waiting for transfers between devices  87.8 us (62%)
  blocking collectives  22 us (15%)
  between operations  14.9 us (10%)
  matrix products  8.46 us (6%)
  local copies, waits for them, and re-layouts  4.9 us (3%)
  other arithmetic  3.62 us (3%)
    reduce_scatter x1, waiting for transfers between devices, local(): lax.psum_scatter(jnp.concatenate([jnp.dot(query_part, query_float, precis...  71.9 us
    psum x1, blocking collectives, local(): total_square = lax.psum(jnp.sum(projected * projected), 'fs')  22 us
    all_gather x1, waiting for transfers between devices, local(): lax.all_gather(jnp.stack([query_projected, key_projected]), 'tp')  15.9 us
    dot_general x1, matrix products, local(): lax.dot_general(normed_input, query_cotangent, contract, preferred_elemen...  3.68 us
    unnamed x23, local copies, waits for them, and re-layouts  3.08 us
  transfers between devices with their start and end apart: 2, of which 2 were waited for; matrix products, arithmetic and copies ran while one was open for 0% of the time, Pallas kernels for 0%

profile of v1, /device:TPU:0, one launch (start us, length us, event | category | flops | bytes accessed | tf_op | source)
XLA Modules:
  0.0 141.8 jit_solution(13027463954613374363)
XLA Ops:
  7.2 0.0 copy-start
  7.2 0.0 copy-start.2
  7.2 0.0 reduce-scatter.2.cloned.1.call-start
  7.2 1.0 copy-done
  8.2 0.0 copy-start.1
  8.2 3.7 %fusion.6 = f32[2048,256]{1,0:T(8,128)S(1)} fusion(bf16[1024,2048]{1,0:T(8,128)(2,1)} %param.9, bf16[1024,256]{1,0:T(8,128)(2,1)S(1)} %copy-done), kind=kOutput, calls=%fused_computation.17 | convolution fusion | flops 1073741824 | bytes 6815744 | tf_op jit(solution)/shard_map/dot_general | solution.py:30
  11.9 0.0 copy-done.2
  11.9 0.0 copy-done.1
  11.9 0.0 copy-start.4
  11.9 1.3 fusion.8
  13.2 0.0 copy-done.4
  13.3 0.0 copy-start.7
  13.3 0.8 fusion.7
  14.1 0.0 copy-done.7
  14.1 0.5 fusion.9
  14.6 1.5 %pad_maximum_fusion = f32[2048,256]{0,1:T(8,128)} fusion(f32[2048,128]{0,1:T(8,128)S(1)} %fusion.9, f32[2048,128]{0,1:T(8,128)S(1)} %fusion.7), kind=kLoop, calls=%fused_computation | loop fusion | flops 524288 | bytes 4194304 | tf_op jit(solution)/shard_map/concatenate | solution.py:38
  16.1 0.0 copy-start.5
  16.1 0.0 reduce-scatter.2.cloned.1.call-update
  16.1 0.0 all-gather.3.cloned.1.call-start
  16.2 71.9 %reduce-scatter.2.cloned.1.call-done = f32[256,256]{0,1:T(8,128)} async-done(((f32[2048,256]{0,1:T(8,128)}), f32[256,256]{0,1:T(8,128)}) %reduce-scatter.2.cloned.1.call-update) | async-done | bytes 262160 | tf_op jit(solution)/shard_map/reduce_scatter | solution.py:37
  88.1 1.0 slice_bitcast_fusion.5
  89.1 0.0 copy-start.6
  89.1 0.8 copy.18
  89.9 0.0 all-gather.3.cloned.1.call-update
  90.0 0.0 copy-done.5
  90.0 0.1 copy.17
  90.1 15.9 %all-gather.3.cloned.1.call-done = f32[8,256,128]{2,1,0:T(8,128)} async-done(((f32[2,256,128]{2,1,0:T(8,128)}), f32[8,256,128]{2,1,0:T(8,128)}) %all-gather.3.cloned.1.call-update) | async-done | bytes 1048592 | tf_op jit(solution)/shard_map/all_gather | solution.py:51
  106.0 0.0 copy-start.3
  106.0 1.3 reduce_sum.18
  107.4 0.0 copy-start.8
  107.4 0.1 copy.23
  107.5 0.7 multiply_reduce_fusion
  108.2 0.0 copy-done.6
  108.2 0.1 copy.20
  108.3 22.0 %psum.7 = f32[]{:T(128)} all-reduce(f32[]{:T(128)} %multiply_reduce_fusion), channel_id=1, replica_groups=mesh['fs'=8,'tp'=4] {'fs'}, use_global_device_ids=true, to_apply=%region_3.0 | all-reduce | flops 1 | bytes 8 | tf_op jit(solution)/shard_map/psum | solution.py:52
  131.0 0.1 rsqrt_multiply_fusion
  131.1 0.0 copy-done.3
  131.1 1.1 fusion.4
  132.2 0.0 copy-done.8
  132.2 1.0 fusion.3
  133.3 0.8 copy.21
  134.1 0.8 copy.22
  (1 shorter events, 0.0 us)
Async XLA Ops:
  7.2 1.0 copy-start
  7.2 4.7 %copy-start.2 = (bf16[1024,128]{1,0:T(8,128)(2,1)S(1)}, bf16[1024,128]{1,0:T(8,128)(2,1)}, u32[]{:S(2)}) copy-start(bf16[1024,128]{1,0:T(8,128)(2,1)} %param.11) | copy-start | bytes 786436
  7.2 80.9 %reduce-scatter.2.cloned.1.call-start = ((), (), s32[]{:S(2)}) async-start(), calls=%async_computation.1 | async-start | bytes 2359296 | tf_op jit(solution)/shard_map/reduce_scatter | solution.py:37
  8.2 3.7 %copy-start.1 = (bf16[1024,2048]{1,0:T(8,128)(2,1)S(1)}, bf16[1024,2048]{1,0:T(8,128)(2,1)}, u32[]{:S(2)}) copy-start(bf16[1024,2048]{1,0:T(8,128)(2,1)} %param.9) | copy-start | bytes 12582916
  11.9 1.3 copy-start.4
  13.3 0.9 copy-start.7
  16.1 73.9 %copy-start.5 = (f32[2,256,128]{2,1,0:T(8,128)S(1)}, f32[2,256,128]{2,1,0:T(8,128)}, u32[]{:S(2)}) copy-start(f32[2,256,128]{2,1,0:T(8,128)} %param.16) | copy-start | bytes 786436
  16.1 89.9 %all-gather.3.cloned.1.call-start = ((), (), s32[]{:S(2)}) async-start(), calls=%async_computation.2 | async-start | bytes 1310720 | tf_op jit(solution)/shard_map/all_gather | solution.py:51
  89.1 19.1 %copy-start.6 = (f32[2,256,128]{2,1,0:T(8,128)S(1)}, f32[2,256,128]{2,1,0:T(8,128)}, u32[]{:S(2)}) copy-start(f32[2,256,128]{2,1,0:T(8,128)} %param.17) | copy-start | bytes 786436
  106.0 25.1 %copy-start.3 = (f32[256,256]{1,0:T(8,128)S(1)}, f32[256,256]{1,0:T(8,128)}, u32[]{:S(2)}) copy-start(f32[256,256]{1,0:T(8,128)} %param.12) | copy-start | bytes 786436
  107.4 24.9 %copy-start.8 = (f32[256,128]{1,0:T(8,128)S(1)}, f32[256,128]{1,0:T(8,128)}, u32[]{:S(2)}) copy-start(f32[256,128]{1,0:T(8,128)} %param.13) | copy-start | bytes 393220
Sparse Core Ops, SparseCore 0:
  16.3 71.7 reduce-scatter.1
  90.2 15.7 all-gather.2
